TPU v7x, 32 devices: a whole 2x2x4 slice. The times are simulated.
32 devices in a mesh: kv: 8 (over z, y), tp: 4 (over x, core).
Axes of the slice: x: 2, y: 2, z: 4, core: 2. Of those that a mesh axis runs over, the one named last changes fastest.
Arguments:
- tokens: bfloat16 [8, 2048], P(None, 'kv'), may hold values from -6 to 6
- in_gain: float32 [2048], P('kv'), may hold values from 0.1 to 1.9
- w_query: bfloat16 [2048, 512], P('kv', 'tp'), may hold values from -0.125 to 0.125
- score_bias: float32 [4], P('tp'), as said below
- cache_keys: bfloat16 [8, 8192, 512], P(None, 'kv', 'tp'), may hold values from -8 to 8, as said below
- cache_values: bfloat16 [8, 8192, 512], P(None, 'kv', 'tp'), may hold values from -6 to 6
- lengths: int32 [8], replicated, may hold values from 1024 to 8192, as said below
- head_gain: float32 [512], P('tp'), may hold values from 0.1 to 1.9
- w_out: bfloat16 [512, 2048], P('tp', 'kv'), may hold values from -0.25 to 0.25
Outputs:
- mixed: bfloat16 [8, 2048], P(None, 'kv')
Inputs may be any that keep to these rules, and one draw needn't show every extreme that they name: `score_bias`: one value a head, added to every score of that head. `cache_keys`: real-valued key entries. `lengths`: one sequence has all 8192 positions cached.
All inputs are finite; a program needn't handle non-finite values.
Results may differ from a plain program's by a relative error of at most 0.0095.
The roundings to bfloat16 on the way count: a program that leaves them out, or rounds other values in their place, can miss the bound.
Values may be sent and summed in bfloat16 or wider, within the bound.
No kernel may reach another device: no remote copies, remote signals or barrier semaphores. Data moves between devices by JAX's collectives and lax.ppermute only.
A program may use at most 64 MiB of HBM per device.

v0:
```python
import jax
import jax.numpy as jnp
from jax import lax
from jax.sharding import PartitionSpec as P

D = 2048
EPS = 1e-06


def shards(
    tokens, in_gain, w_query, score_bias, cache_keys, cache_values, lengths, head_gain, w_out
):
    sequences = tokens.shape[0]
    local_len = cache_keys.shape[1]
    head_width = cache_keys.shape[2]
    heads_here = score_bias.shape[0]
    head_size = head_width // heads_here
    as_float = tokens.astype(jnp.float32)
    gained = (as_float * in_gain).astype(jnp.bfloat16)
    partial_value = jnp.dot(gained, w_query, preferred_element_type=jnp.float32)
    squares = jnp.sum(as_float * as_float, axis=1)
    summed, total_sq = lax.psum((partial_value, squares), "kv")
    row_scale = lax.rsqrt(total_sq / D + EPS)
    queries = (
        (summed * row_scale[:, None]).astype(jnp.bfloat16).reshape(sequences, heads_here, head_size)
    )
    key_heads = cache_keys.reshape(sequences, local_len, heads_here, head_size)
    value_heads = cache_values.reshape(sequences, local_len, heads_here, head_size)
    scores = jnp.einsum("bhd,bphd->bhp", queries, key_heads, preferred_element_type=jnp.float32)
    scores = scores * head_size ** (-0.5) + score_bias[None, :, None]
    offset = lax.axis_index("kv") * local_len
    places = offset + lax.iota(jnp.int32, local_len)
    usable = places[None, None, :] < lengths[:, None, None]
    log_keep = jnp.where(usable, jax.nn.log_sigmoid(-scores), 0.0)
    strict_upper = (
        lax.iota(jnp.int32, local_len)[:, None] > lax.iota(jnp.int32, local_len)[None, :]
    ).astype(jnp.float32)
    suffix = jnp.einsum("bhr,rs->bhs", log_keep, strict_upper, precision=lax.Precision.HIGHEST)
    weights = jnp.where(usable, jnp.exp(jax.nn.log_sigmoid(scores) + suffix), 0.0).astype(
        jnp.bfloat16
    )
    local_out = jnp.einsum(
        "bhp,bphd->bhd", weights, value_heads, preferred_element_type=jnp.float32
    )
    seg_total = jnp.sum(log_keep, axis=2)
    every_total = lax.all_gather(seg_total[None], "kv", axis=0, tiled=True)
    ranks_kv = lax.iota(jnp.int32, every_total.shape[0])
    later_sum = jnp.sum(
        jnp.where((ranks_kv > lax.axis_index("kv"))[:, None, None], every_total, 0.0), axis=0
    )
    attended = lax.psum(local_out * jnp.exp(later_sum)[..., None], "kv")
    mean_sq = jnp.mean(attended * attended, axis=2)
    normed = attended * lax.rsqrt(mean_sq + EPS)[..., None]
    normed = (normed.reshape(sequences, head_width) * head_gain).astype(jnp.bfloat16)
    part_out = jnp.dot(normed, w_out, preferred_element_type=jnp.float32)
    return lax.psum(part_out.astype(jnp.bfloat16), "tp")


def solution(mesh):
    return jax.shard_map(
        shards,
        mesh=mesh,
        in_specs=(
            P(None, "kv"),
            P("kv"),
            P("kv", "tp"),
            P("tp"),
            P(None, "kv", "tp"),
            P(None, "kv", "tp"),
            P(),
            P("tp"),
            P("tp", "kv"),
        ),
        out_specs=P(None, "kv"),
        check_vma=False,
    )
```

profile of v0, /device:TPU:0, one launch (start us, length us, event | category | flops | bytes accessed | tf_op | source)
XLA Modules:
  0.0 74.4 jit_solution(1985934041813011728)
XLA Ops:
  0.0 0.0 copy-start
  0.0 1.2 %fusion.19 = f32[8,128]{1,0:T(8,128)S(1)} fusion(bf16[256,128]{1,0:T(8,128)(2,1)} %param.11, bf16[8,256]{1,0:T(8,128)(2,1)} %param.9, f32[256]{0:T(256)} %param.10), kind=kOutput, calls=%fused_computation.27 | convolution fusion | flops 530432 | bytes 74752 | tf_op jit(solution)/shard_map/dot_general | solution.py:20
  1.2 0.8 %fusion.18 = f32[8]{0:T(128)S(1)} fusion(bf16[8,256]{1,0:T(8,128)(2,1)} %param.9), kind=kLoop, calls=%fused_computation.26 | loop fusion | flops 6136 | bytes 4128 | tf_op jit(solution)/shard_map/reduce_sum | solution.py:21
  2.0 23.4 %all-reduce.1 = (f32[8,128]{1,0:T(8,128)S(1)}, f32[8]{0:T(128)S(1)}) all-reduce(f32[8,128]{1,0:T(8,128)S(1)} %fusion.19, f32[8]{0:T(128)S(1)} %fusion.18), channel_id=1, replica_groups=mesh['kv'=8,'tp'=4] {'kv'}, use_global_device_ids=true, to_apply=%region_0.0 | all-reduce | flops 1032 | bytes 8256 | tf_op jit(solution)/shard_map/psum | solution.py:22
  25.4 0.1 fusion.25
  25.5 0.0 copy-done
  25.5 0.6 fusion.22
  26.8 0.0 copy-done.1
  26.8 0.2 fusion.11
  27.0 0.0 copy-done.4
  27.0 0.7 dynamic-slice
  28.4 0.2 dynamic-update-slice
  28.6 17.1 %all-reduce = f32[64]{0:T(128)S(1)} all-reduce(f32[64]{0:T(128)S(1)} %dynamic-update-slice), channel_id=2, replica_groups=mesh['kv'=8,'tp'=4] {'kv'}, use_global_device_ids=true, to_apply=%add | all-reduce | flops 64 | bytes 512
  45.7 0.1 reshape.93
  45.8 0.1 select_reduce_fusion
  45.9 0.7 fusion.5
  46.7 2.0 %fusion.9 = f32[8,1,128]{2,1,0:T(1,128)S(1)} fusion(bf16[8,1024,128]{2,1,0:T(8,128)(2,1)} %param.14, bf16[8,1024,1]{1,0,2:T(8,128)(2,1)S(1)} %fusion.5), kind=kOutput, calls=%fused_computation.15 | convolution fusion | flops 2097152 | bytes 2117632 | tf_op jit(solution)/shard_map/bhp,bphd->bhd/dot_general | solution.py:42
  48.6 0.1 multiply_bitcast_fusion
  48.7 19.1 %psum.30 = f32[8,1,128]{2,0,1:T(8,128)S(1)} all-reduce(f32[8,1,128]{2,0,1:T(8,128)S(1)} %multiply_bitcast_fusion), channel_id=1, replica_groups=mesh['kv'=8,'tp'=4] {'kv'}, use_global_device_ids=true, to_apply=%region_5.6 | all-reduce | flops 1024 | bytes 8192 | tf_op jit(solution)/shard_map/psum | solution.py:51
  67.8 0.1 multiply_reduce_fusion
  68.0 0.0 copy-done.2
  68.0 0.0 copy-done.3
  68.0 0.2 convolution_convert_fusion
  68.2 6.2 %psum.31 = bf16[8,256]{1,0:T(8,128)(2,1)} all-reduce(bf16[8,256]{1,0:T(8,128)(2,1)S(1)} %convolution_convert_fusion), channel_id=1, replica_groups=mesh['kv'=8,'tp'=4] {'tp'}, use_global_device_ids=true, to_apply=%region_7.8 | all-reduce | flops 2048 | bytes 8192 | tf_op jit(solution)/shard_map/psum | solution.py:56
  (10 shorter events, 0.0 us)
Async XLA Ops:
  0.0 25.5 %copy-start = (bf16[8,1024,128]{2,1,0:T(8,128)(2,1)S(1)}, bf16[8,1024,128]{2,1,0:T(8,128)(2,1)}, u32[]{:S(2)}) copy-start(bf16[8,1024,128]{2,1,0:T(8,128)(2,1)} %param.13) | copy-start | bytes 6291460
  0.0 27.0 %copy-start.4 = (u32[32]{0:T(128)S(1)}, u32[32]{0:T(128)}, u32[]{:S(2)}) copy-start(u32[32]{0:T(128)} %constant.28) | copy-start | bytes 388
  0.0 26.8 %copy-start.1 = (s32[8]{0:T(128)S(1)}, s32[8]{0:T(128)}, u32[]{:S(2)}) copy-start(s32[8]{0:T(128)} %param.15) | copy-start | bytes 100
  26.1 41.9 %copy-start.2 = (bf16[128,256]{1,0:T(8,128)(2,1)S(1)}, bf16[128,256]{1,0:T(8,128)(2,1)}, u32[]{:S(2)}) copy-start(bf16[128,256]{1,0:T(8,128)(2,1)} %param.17) | copy-start | bytes 196612
  26.1 41.9 %copy-start.3 = (f32[128]{0:T(128)S(1)}, f32[128]{0:T(128)}, u32[]{:S(2)}) copy-start(f32[128]{0:T(128)} %param.16) | copy-start | bytes 1540
where the time goes:
time: 74.7 us; the launch traced here: 74.4 us
  blocking collectives  65.9 us (88%)
  matrix products  4.69 us (6%)
  between operations  1.47 us (2%)
  other arithmetic  1.37 us (2%)
  local copies, waits for them, and re-layouts  1.01 us (1%)
    psum x1, blocking collectives, shards(): summed, total_sq = lax.psum((partial_value, squares), 'kv')  23.4 us
    psum x1, blocking collectives, shards(): attended = lax.psum(local_out * jnp.exp(later_sum)[..., None], 'kv')  19.1 us
    unnamed x1, blocking collectives  17.1 us
    psum x1, blocking collectives, shards(): return lax.psum(part_out.astype(jnp.bfloat16), 'tp')  6.23 us
    dot_general x1, matrix products, shards(): jnp.einsum('bhp,bphd->bhd', weights, value_heads, preferred_element_type=...  1.98 us

commit v1 on v0

--- a/solution.py
+++ b/solution.py
@@ -48,7 +48,9 @@
     later_sum = jnp.sum(
         jnp.where((ranks_kv > lax.axis_index("kv"))[:, None, None], every_total, 0.0), axis=0
     )
-    attended = lax.psum(local_out * jnp.exp(later_sum)[..., None], "kv")
+    own = local_out * jnp.exp(later_sum)[..., None]
+    terms = lax.all_gather(own, "kv", axis=0, tiled=False)
+    attended = terms.sum(axis=0)
     mean_sq = jnp.mean(attended * attended, axis=2)
     normed = attended * lax.rsqrt(mean_sq + EPS)[..., None]
     normed = (normed.reshape(sequences, head_width) * head_gain).astype(jnp.bfloat16)

time: 74.7 us -> 86.2 us (1.15)
  blocking collectives: 65.9 us -> 77.3 us
    all_gather x0 -> x1, blocking collectives: none -> 30.6 us  [shards(): terms = lax.all_gather(own, 'kv', axis=0, tiled=False)]
    psum x1 -> x0, blocking collectives: 19.1 us -> none  [shards(): attended = lax.psum(local_out * jnp.exp(later_sum)[..., None], 'kv')]
where the time goes in v1:
time: 86.2 us; the launch traced here: 85.9 us
  blocking collectives  77.3 us (90%)
  matrix products  4.69 us (5%)
  between operations  1.47 us (2%)
  other arithmetic  1.38 us (2%)
  local copies, waits for them, and re-layouts  1.01 us (1%)
    all_gather x1, blocking collectives, shards(): terms = lax.all_gather(own, 'kv', axis=0, tiled=False)  30.6 us
    psum x1, blocking collectives, shards(): summed, total_sq = lax.psum((partial_value, squares), 'kv')  23.4 us
    unnamed x1, blocking collectives  17.1 us
    psum x1, blocking collectives, shards(): return lax.psum(part_out.astype(jnp.bfloat16), 'tp')  6.23 us
    dot_general x1, matrix products, shards(): jnp.einsum('bhp,bphd->bhd', weights, value_heads, preferred_element_type=...  1.98 us

profile of v1, /device:TPU:0, one launch (start us, length us, event | category | flops | bytes accessed | tf_op | source)
XLA Modules:
  0.0 85.9 jit_solution(12941498199451985340)
XLA Ops:
  0.0 0.0 copy-start
  0.0 1.2 %fusion.19 = f32[8,128]{1,0:T(8,128)S(1)} fusion(bf16[256,128]{1,0:T(8,128)(2,1)} %param.11, bf16[8,256]{1,0:T(8,128)(2,1)} %param.9, f32[256]{0:T(256)} %param.10), kind=kOutput, calls=%fused_computation.28 | convolution fusion | flops 530432 | bytes 74752 | tf_op jit(solution)/shard_map/dot_general | solution.py:20
  1.2 0.8 fusion.18
  2.0 23.4 %all-reduce.1 = (f32[8,128]{1,0:T(8,128)S(1)}, f32[8]{0:T(128)S(1)}) all-reduce(f32[8,128]{1,0:T(8,128)S(1)} %fusion.19, f32[8]{0:T(128)S(1)} %fusion.18), channel_id=1, replica_groups=mesh['kv'=8,'tp'=4] {'kv'}, use_global_device_ids=true, to_apply=%region_0.0 | all-reduce | flops 1032 | bytes 8256 | tf_op jit(solution)/shard_map/psum | solution.py:22
  25.4 0.1 fusion.24
  25.5 0.0 copy-done
  25.5 0.6 fusion.21
  26.8 0.0 copy-done.1
  26.8 0.2 fusion.11
  27.0 0.0 copy-done.4
  27.0 0.7 dynamic-slice
  28.4 0.2 dynamic-update-slice
  28.6 17.1 %all-reduce = f32[64]{0:T(128)S(1)} all-reduce(f32[64]{0:T(128)S(1)} %dynamic-update-slice), channel_id=2, replica_groups=mesh['kv'=8,'tp'=4] {'kv'}, use_global_device_ids=true, to_apply=%add | all-reduce | flops 64 | bytes 512
  45.7 0.1 reshape.106
  45.8 0.1 select_reduce_fusion
  45.9 0.7 fusion.5
  46.7 2.0 %fusion.9 = f32[8,1,128]{2,1,0:T(1,128)S(1)} fusion(bf16[8,1024,128]{2,1,0:T(8,128)(2,1)} %param.14, bf16[8,1024,1]{1,0,2:T(8,128)(2,1)S(1)} %fusion.5), kind=kOutput, calls=%fused_computation.16 | convolution fusion | flops 2097152 | bytes 2117632 | tf_op jit(solution)/shard_map/bhp,bphd->bhd/dot_general | solution.py:42
  48.6 0.1 broadcast_multiply_fusion
  48.7 30.6 %all-gather.1 = f32[64,128]{1,0:T(8,128)S(1)} all-gather(f32[8,128]{1,0:T(8,128)S(1)} %broadcast_multiply_fusion), channel_id=3, replica_groups=mesh['kv'=8,'tp'=4] {'kv'}, dimensions={0}, use_global_device_ids=true | all-gather | bytes 36864 | tf_op jit(solution)/shard_map/all_gather | solution.py:52
  79.3 0.1 multiply_reduce_fusion
  79.5 0.0 copy-done.2
  79.5 0.0 copy-done.3
  79.5 0.2 convolution_convert_fusion
  79.7 6.2 %psum.23 = bf16[8,256]{1,0:T(8,128)(2,1)} all-reduce(bf16[8,256]{1,0:T(8,128)(2,1)S(1)} %convolution_convert_fusion), channel_id=1, replica_groups=mesh['kv'=8,'tp'=4] {'tp'}, use_global_device_ids=true, to_apply=%region_7.8 | all-reduce | flops 2048 | bytes 8192 | tf_op jit(solution)/shard_map/psum | solution.py:58
  (11 shorter events, 0.0 us)
Async XLA Ops:
  0.0 25.5 %copy-start = (bf16[8,1024,128]{2,1,0:T(8,128)(2,1)S(1)}, bf16[8,1024,128]{2,1,0:T(8,128)(2,1)}, u32[]{:S(2)}) copy-start(bf16[8,1024,128]{2,1,0:T(8,128)(2,1)} %param.13) | copy-start | bytes 6291460
  0.0 27.0 %copy-start.4 = (u32[32]{0:T(128)S(1)}, u32[32]{0:T(128)}, u32[]{:S(2)}) copy-start(u32[32]{0:T(128)} %constant.28) | copy-start | bytes 388
  0.0 26.8 %copy-start.1 = (s32[8]{0:T(128)S(1)}, s32[8]{0:T(128)}, u32[]{:S(2)}) copy-start(s32[8]{0:T(128)} %param.15) | copy-start | bytes 100
  26.1 53.4 %copy-start.2 = (bf16[128,256]{1,0:T(8,128)(2,1)S(1)}, bf16[128,256]{1,0:T(8,128)(2,1)}, u32[]{:S(2)}) copy-start(bf16[128,256]{1,0:T(8,128)(2,1)} %param.17) | copy-start | bytes 196612
  26.1 53.4 %copy-start.3 = (f32[128]{0:T(128)S(1)}, f32[128]{0:T(128)}, u32[]{:S(2)}) copy-start(f32[128]{0:T(128)} %param.16) | copy-start | bytes 1540
